TPU v7x, 32 devices: a whole 2x2x4 slice. The times are simulated.
32 devices in a mesh: rep: 4 (over z), fs: 4 (over y, x), tp: 2 (over core).
Axes of the slice: x: 2, y: 2, z: 4, core: 2. Of those that a mesh axis runs over, the one named last changes fastest.
Arguments:
- hidden_in: bfloat16 [2048, 2048], P('rep'), may hold values from -6 to 6
- cotangent: bfloat16 [2048, 2048], P('rep'), may hold values from -3 to 3
- w_up: bfloat16 [2048, 8192], P('rep', ('fs', 'tp')), may hold values from -0.125 to 0.125
- w_down: bfloat16 [8192, 2048], P(('fs', 'tp'), 'rep'), may hold values from -0.0625 to 0.0625
Outputs:
- input_grad: bfloat16 [2048, 2048], P('rep')
- up_grad: float32 [2048, 8192], P('rep', ('fs', 'tp'))
- down_grad: float32 [8192, 2048], P(('fs', 'tp'), 'rep')
All inputs are finite; a program needn't handle non-finite values.
Results may differ from a plain program's by a relative error of at most 0.017.
Values may be sent and summed in bfloat16 or wider, within the bound.
A program may use at most 64 MiB of HBM per device.

v0:
```python
import jax
import jax.numpy as jnp
from jax import lax
from jax.sharding import PartitionSpec as P


def contract_last(left, right):
    return lax.dot_general(
        left, right, (((1,), (1,)), ((), ())), preferred_element_type=jnp.float32
    )


def contract_first(left, right):
    return lax.dot_general(
        left, right, (((0,), (0,)), ((), ())), preferred_element_type=jnp.float32
    )


def on_device(hidden_in, cotangent, w_up, w_down):
    up_full = lax.all_gather(w_up, "rep", axis=0, tiled=True)
    back_grad = contract_last(cotangent, lax.all_gather(w_down, "rep", axis=1, tiled=True))
    preact = jnp.dot(hidden_in, up_full, preferred_element_type=jnp.float32)
    active = jnp.maximum(preact, 0.0)
    hidden = (active * active).astype(jnp.bfloat16)
    slopes = (2.0 * active * back_grad).astype(jnp.bfloat16)
    grad_upper = lax.psum_scatter(
        contract_first(hidden_in, slopes).astype(jnp.bfloat16),
        "rep",
        scatter_dimension=0,
        tiled=True,
    ).astype(jnp.float32)
    lower_rows = lax.psum_scatter(
        contract_first(cotangent, hidden).astype(jnp.bfloat16),
        "rep",
        scatter_dimension=0,
        tiled=True,
    ).astype(jnp.float32)
    down_grad = lower_rows.T
    partial_sum = contract_last(slopes, up_full).astype(jnp.bfloat16)
    input_grad = lax.psum(partial_sum, ("fs", "tp")).astype(jnp.float32).astype(jnp.bfloat16)
    return (input_grad, grad_upper, down_grad)


def solution(mesh):
    return jax.shard_map(
        on_device,
        mesh=mesh,
        in_specs=(P("rep", None), P("rep", None), P("rep", ("fs", "tp")), P(("fs", "tp"), "rep")),
        out_specs=(P("rep", None), P("rep", ("fs", "tp")), P(("fs", "tp"), "rep")),
        check_vma=False,
    )
```

profile of v0, /device:TPU:25, one launch (start us, length us, event | category | flops | bytes accessed | tf_op | source)
XLA Modules:
  0.0 411.8 jit_solution(14841434194789787365)
XLA Ops:
  7.2 0.0 copy-start
  7.2 0.0 all-gather.3.cloned.1.call-start
  7.2 0.7 all-gather.3.cloned.1.call-update
  7.9 0.0 all-gather.5.cloned.1.call-start
  8.0 0.7 all-gather.5.cloned.1.call-update
  8.7 0.0 reduce-scatter.3.cloned.1.call-start
  8.7 80.0 %all-gather.3.cloned.1.call-done = bf16[2048,1024]{1,0:T(8,128)(2,1)} async-done(((bf16[512,1024]{1,0:T(8,128)(2,1)}), bf16[2048,1024]{1,0:T(8,128)(2,1)}) %all-gather.3.cloned.1.call-update) | async-done | bytes 4194320 | tf_op jit(solution)/shard_map/all_gather | solution.py:20
  88.7 0.0 copy-done
  88.7 5.8 %fusion.2 = f32[512,1024]{1,0:T(8,128)} fusion(bf16[512,2048]{1,0:T(8,128)(2,1)S(1)} %copy-done, bf16[2048,1024]{1,0:T(8,128)(2,1)} %all-gather.3.cloned.1.call-done), kind=kOutput, calls=%fused_computation.8 | convolution fusion | flops 2147483648 | bytes 8388608 | tf_op jit(solution)/shard_map/dot_general | solution.py:22
  94.6 75.0 %all-gather.5.cloned.1.call-done = bf16[1024,2048]{1,0:T(8,128)(2,1)} async-done(((bf16[1024,512]{1,0:T(8,128)(2,1)}), bf16[1024,2048]{1,0:T(8,128)(2,1)}) %all-gather.5.cloned.1.call-update) | async-done | bytes 4194320 | tf_op jit(solution)/shard_map/all_gather | solution.py:21
  169.6 5.8 %multiply_convert_fusion.1 = bf16[512,1024]{1,0:T(8,128)(2,1)S(1)} fusion(f32[512,1024]{1,0:T(8,128)} %fusion.2, bf16[512,2048]{1,0:T(8,128)(2,1)} %param.5, bf16[1024,2048]{1,0:T(8,128)(2,1)} %all-gather.5.cloned.1.call-done), kind=kOutput, calls=%fused_computation.5 | convolution fusion | flops 2149580800 | bytes 9437184 | tf_op jit(solution)/shard_map/dot_general | solution.py:8
  175.4 4.4 %convert_bitcast_fusion.1 = bf16[2048,1024]{0,1:T(8,128)(2,1)} fusion(bf16[512,1024]{1,0:T(8,128)(2,1)S(1)} %multiply_convert_fusion.1, bf16[512,2048]{1,0:T(8,128)(2,1)S(1)} %copy-done), kind=kOutput, calls=%fused_computation.1 | convolution fusion | flops 2149580800 | bytes 7340032 | tf_op jit(solution)/shard_map/dot_general | solution.py:14
  179.8 0.0 reduce-scatter.3.cloned.1.call-update
  179.8 0.0 reduce-scatter.5.cloned.1.call-start
  179.9 6.6 %convert_bitcast_fusion = bf16[2048,1024]{0,1:T(8,128)(2,1)} fusion(bf16[512,2048]{1,0:T(8,128)(2,1)} %param.5, f32[512,1024]{1,0:T(8,128)} %fusion.2), kind=kOutput, calls=%fused_computation | convolution fusion | flops 2151153664 | bytes 8388608 | tf_op jit(solution)/shard_map/dot_general | solution.py:14
  186.4 0.0 reduce-scatter.5.cloned.1.call-update
  186.5 0.0 all-reduce.2.cloned.1.call-start
  186.5 6.7 %convolution_convert_fusion = bf16[512,2048]{1,0:T(8,128)(2,1)} fusion(bf16[512,1024]{1,0:T(8,128)(2,1)S(1)} %multiply_convert_fusion.1, bf16[2048,1024]{1,0:T(8,128)(2,1)} %all-gather.3.cloned.1.call-done), kind=kOutput, calls=%fused_computation.2 | convolution fusion | flops 2148532224 | bytes 7340032 | tf_op jit(solution)/shard_map/dot_general | solution.py:8
  193.2 0.0 all-reduce.2.cloned.1.call-update
  193.2 64.0 %reduce-scatter.3.cloned.1.call-done = bf16[512,1024]{0,1:T(8,128)(2,1)} async-done(((bf16[2048,1024]{0,1:T(8,128)(2,1)}), bf16[512,1024]{0,1:T(8,128)(2,1)}) %reduce-scatter.3.cloned.1.call-update) | async-done | bytes 1048592 | tf_op jit(solution)/shard_map/reduce_scatter | solution.py:26
  257.2 2.6 copy.7
  259.8 76.9 %reduce-scatter.5.cloned.1.call-done = bf16[512,1024]{0,1:T(8,128)(2,1)} async-done(((bf16[2048,1024]{0,1:T(8,128)(2,1)}), bf16[512,1024]{0,1:T(8,128)(2,1)}) %reduce-scatter.5.cloned.1.call-update) | async-done | bytes 1048592 | tf_op jit(solution)/shard_map/reduce_scatter | solution.py:32
  336.7 2.8 convert_bitcast_fusion.2
  339.5 62.6 %all-reduce.2.cloned.1.call-done = bf16[512,2048]{1,0:T(8,128)(2,1)} async-done(((bf16[512,2048]{1,0:T(8,128)(2,1)}), bf16[512,2048]{1,0:T(8,128)(2,1)}) %all-reduce.2.cloned.1.call-update) | async-done | bytes 2097168 | tf_op jit(solution)/shard_map/psum | solution.py:40
  402.1 3.2 copy.9
Async XLA Ops:
  7.2 81.6 %copy-start = (bf16[512,2048]{1,0:T(8,128)(2,1)S(1)}, bf16[512,2048]{1,0:T(8,128)(2,1)}, u32[]{:S(2)}) copy-start(bf16[512,2048]{1,0:T(8,128)(2,1)} %param.4) | copy-start | bytes 6291460
  7.2 81.5 %all-gather.3.cloned.1.call-start = ((), (), s32[]{:S(2)}) async-start(), calls=%async_computation.2 | async-start | bytes 5242880 | tf_op jit(solution)/shard_map/all_gather | solution.py:20
  7.9 161.6 %all-gather.5.cloned.1.call-start = ((), (), s32[]{:S(2)}) async-start(), calls=%async_computation.3 | async-start | bytes 5242880 | tf_op jit(solution)/shard_map/all_gather | solution.py:21
  8.7 248.5 %reduce-scatter.3.cloned.1.call-start = ((), (), s32[]{:S(2)}) async-start(), calls=%async_computation.5 | async-start | bytes 5242880 | tf_op jit(solution)/shard_map/reduce_scatter | solution.py:26
  179.8 156.9 %reduce-scatter.5.cloned.1.call-start = ((), (), s32[]{:S(2)}) async-start(), calls=%async_computation.6 | async-start | bytes 5242880 | tf_op jit(solution)/shard_map/reduce_scatter | solution.py:32
  186.5 215.6 %all-reduce.2.cloned.1.call-start = ((), (), s32[]{:S(2)}) async-start(), calls=%async_computation.4 | async-start | bytes 4194304 | tf_op jit(solution)/shard_map/psum | solution.py:40
Sparse Core Ops, SparseCore 0:
  9.6 79.1 all-gather.2
  90.3 79.2 all-gather.4
  179.9 77.2 reduce-scatter.2
  259.4 77.2 reduce-scatter.4
  340.3 61.6 all-reduce.1
where the time goes:
time: 415 us; the launch traced here: 412 us
  waiting for transfers between devices  360 us (87%)
  matrix products  29.3 us (7%)
  between operations  13.8 us (3%)
  local copies, waits for them, and re-layouts  5.73 us (1%)
    all_gather x1, waiting for transfers between devices, on_device(): up_full = lax.all_gather(w_up, 'rep', axis=0, tiled=True)  80 us
    reduce_scatter x1, waiting for transfers between devices, on_device(): lax.psum_scatter(contract_first(cotangent, hidden).astype(jnp.bfloat16),...  76.9 us
    all_gather x1, waiting for transfers between devices, on_device(): lax.all_gather(w_down, 'rep', axis=1, tiled=True)  75 us
    reduce_scatter x1, waiting for transfers between devices, on_device(): lax.psum_scatter(contract_first(hidden_in, slopes).astype(jnp.bfloat16),...  64 us
    psum x1, waiting for transfers between devices, on_device(): lax.psum(partial_sum, ('fs', 'tp')).astype(jnp.float32).astype(jnp.bfloat16)  62.6 us
    dot_general x2, matrix products, contract_last(): lax.dot_general(left, right, (((1,), (1,)), ((), ())), preferred_element_...  12.5 us
    dot_general x2, matrix products, contract_first(): lax.dot_general(left, right, (((0,), (0,)), ((), ())), preferred_element_...  10.9 us
  transfers between devices with their start and end apart: 5, of which 5 were waited for; matrix products, arithmetic and copies ran while one was open for 6% of the time, Pallas kernels for 0%

commit v1 on v0

v1 whole, which is shorter than its diff:
```python
import functools

import jax
import jax.numpy as jnp
from jax import lax
from jax.experimental import pallas as pl
from jax.experimental.pallas import tpu as pltpu
from jax.sharding import PartitionSpec as P

MESH = pl.DeviceIdType.MESH
BF16, F32 = jnp.bfloat16, jnp.float32


def contract_last(left, right):
    return lax.dot_general(left, right, (((1,), (1,)), ((), ())), preferred_element_type=F32)


def contract_first(left, right):
    return lax.dot_general(left, right, (((0,), (0,)), ((), ())), preferred_element_type=F32)


def plain(hidden_in, cotangent, w_up, w_down):
    up_full = lax.all_gather(w_up, "rep", axis=0, tiled=True)
    back_grad = contract_last(cotangent, lax.all_gather(w_down, "rep", axis=1, tiled=True))
    preact = jnp.dot(hidden_in, up_full, preferred_element_type=F32)
    active = jnp.maximum(preact, 0.0)
    hidden = (active * active).astype(BF16)
    slopes = (2.0 * active * back_grad).astype(BF16)
    grad_upper = lax.psum_scatter(
        contract_first(hidden_in, slopes).astype(BF16), "rep", scatter_dimension=0, tiled=True
    ).astype(F32)
    lower_rows = lax.psum_scatter(
        contract_first(cotangent, hidden).astype(BF16), "rep", scatter_dimension=0, tiled=True
    ).astype(F32)
    partial_sum = contract_last(slopes, up_full).astype(BF16)
    input_grad = lax.psum(partial_sum, ("fs", "tp")).astype(F32).astype(BF16)
    return (input_grad, grad_upper, lower_rows.T)


SEMS = 256


def kernel(
    R, x_ref, g_ref, wu_in, wd_in,
    ig_ref, ru_ref, rd_ref,
    tx, tg, wu, wd, act, slopes, s_t, h_t, part, r0, r1, r2, r3, ug, dg,
    send_sems, recv_sems, local_sems,
):
    z, f, c = lax.axis_index("rep"), lax.axis_index("fs"), lax.axis_index("tp")
    tl, D = x_ref.shape
    dl, fl = wu_in.shape
    h = fl // R
    pr = tl // 8
    xx, yy = lax.rem(f, 2), lax.div(f, 2)
    fx, fy = yy * 2 + (1 - xx), (1 - yy) * 2 + xx
    f1 = fx * (1 - c) + fy * c
    f2 = fy * (1 - c) + fx * c
    f3 = 3 - f
    order = [d for d in (1, 3, 2) if d < R] if R == 4 else list(range(1, R))

    pending = []
    keys = {}

    def key_of(key):
        return keys.setdefault(key, len(keys))

    def dev(zz=None, ff=None, cc=None):
        return {"rep": z if zz is None else zz, "fs": f if ff is None else ff, "tp": c if cc is None else cc}

    def send(src, dst, device, key):
        copy = pltpu.make_async_remote_copy(
            src_ref=src, dst_ref=dst, send_sem=send_sems.at[len(pending)],
            recv_sem=recv_sems.at[key_of(key)], device_id=device, device_id_type=MESH)
        copy.start()
        pending.append(copy)

    def arrived(dst, key):
        pltpu.make_async_remote_copy(
            src_ref=dst, dst_ref=dst, send_sem=send_sems.at[0],
            recv_sem=recv_sems.at[key_of(key)], device_id=dev(cc=1 - c), device_id_type=MESH).wait_recv()

    def plane(d):
        return lax.rem(z + d, R)

    def rows(zz, ff, cc):
        return pl.ds(pl.multiple_of(zz * tl + (cc * 4 + ff) * pr, pr), pr)

    barrier = pltpu.get_barrier_semaphore()
    near = [dev(zz=plane(d)) for d in range(1, R)] + [dev(ff=fx), dev(ff=fy), dev(cc=1 - c)]
    for device in near:
        pl.semaphore_signal(barrier, inc=1, device_id=device, device_id_type=MESH)
    pl.semaphore_wait(barrier, len(near))

    tokens = (tx, tg)
    sources = (x_ref, g_ref)

    def send_tokens(a):
        for d in order:
            send(sources[a].at[pl.ds(pl.multiple_of((c * 4 + f) * pr, pr), pr), :],
                 tokens[a].at[rows(z, f, c), :], dev(zz=plane(d)), ("tok", a, R - d, 0))

    def up_cols(zz):
        return pl.ds(pl.multiple_of(zz * h, h), h)

    def d_block(zz):
        return pl.ds(pl.multiple_of(zz * dl, dl), dl)

    send_tokens(0)
    send_tokens(1)
    for d in order:
        send(wu_in.at[:, up_cols(plane(d))], wu.at[d_block(z), :], dev(zz=plane(d)), ("wu", R - d))
    for d in order:
        send(wd_in.at[up_cols(plane(d)), :], wd.at[:, d_block(z)], dev(zz=plane(d)), ("wd", R - d))

    own_rows = pl.ds(pl.multiple_of(z * tl, tl), tl)
    local = [
        pltpu.make_async_copy(x_ref, tx.at[own_rows, :], local_sems.at[0]),
        pltpu.make_async_copy(g_ref, tg.at[own_rows, :], local_sems.at[1]),
        pltpu.make_async_copy(wu_in.at[:, up_cols(z)], wu.at[d_block(z), :], local_sems.at[2]),
        pltpu.make_async_copy(wd_in.at[up_cols(z), :], wd.at[:, d_block(z)], local_sems.at[3]),
    ]
    for copy in local:
        copy.start()

    def spread(buf, tag, zz):
        def piece(ff, cc):
            return buf.at[rows(zz, ff, cc) if zz is not None else
                          pl.ds(pl.multiple_of((cc * 4 + ff) * pr, pr), pr), :]

        def first():
            mine = piece(f, c)
            send(mine, mine, dev(ff=f1), tag + (1,))
            send(mine, mine, dev(ff=f2), tag + (2,))
            send(mine, mine, dev(cc=1 - c), tag + (4,))

        def second():
            p1, p2 = piece(f1, c), piece(f2, c)
            arrived(p1, tag + (1,))
            send(p1, p1, dev(ff=f2), tag + (3,))
            send(p1, p1, dev(cc=1 - c), tag + (5,))
            arrived(p2, tag + (2,))
            send(p2, p2, dev(cc=1 - c), tag + (6,))

        def third():
            p3 = piece(f3, c)
            arrived(p3, tag + (3,))
            send(p3, p3, dev(cc=1 - c), tag + (7,))

        def last():
            for k, ff in ((4, f), (5, f2), (6, f1), (7, f3)):
                arrived(piece(ff, 1 - c), tag + (k,))

        return first, second, third, last

    lasts = {}
    items = [(a, d) for a in (0, 1) for d in order]
    stages = []
    for a, d in items:
        first, second, third, last = spread(tokens[a], ("tok", a, d), plane(d))

        def opening(a=a, d=d, first=first):
            arrived(tokens[a].at[rows(plane(d), f, c), :], ("tok", a, d, 0))
            first()

        stages.append((opening, second, third))
        lasts[a, d] = last
    for i in range(len(items) + 2):
        for back in (0, 1, 2):
            if 0 <= i - back < len(items):
                stages[i - back][back]()

    for copy in local:
        copy.wait()
    for d in order:
        arrived(wu.at[d_block(plane(d)), :], ("wu", d))
    step = min(tl, 256)

    def up_block(d):
        @pl.loop(0, tl // step)
        def _(i):
            at = pl.ds(pl.multiple_of(plane(d) * tl + i * step, step), step)
            active = jnp.maximum(jnp.dot(tx[at, :], wu[...], preferred_element_type=F32), 0.0)
            act[at, :] = active
            h_t[:, at] = jnp.transpose(active * active).astype(BF16)

    up_block(0)
    for d in order:
        lasts[0, d]()
        up_block(d)
    for d in order:
        lasts[1, d]()

    for d in order + [0]:
        at = d_block(plane(d))
        dg[:, at] = jnp.dot(h_t[...], tg[:, at], preferred_element_type=F32).astype(BF16)
        if d:
            send(dg.at[:, at], rd_ref.at[up_cols(z), :], dev(zz=plane(d)), ("rd", R - d))
        else:
            rd_ref[up_cols(z), :] = dg[:, at]

    for d in order:
        arrived(wd.at[:, d_block(plane(d))], ("wd", d))

    def slope_block(d):
        @pl.loop(0, tl // step)
        def _(i):
            at = pl.ds(pl.multiple_of(plane(d) * tl + i * step, step), step)
            value = 2.0 * act[at, :] * contract_last(tg[at, :], wd[...])
            slopes[at, :] = value.astype(BF16)
            s_t[:, at] = jnp.transpose(value).astype(BF16)

    half = 4 * pr

    def half_rows(d, cc):
        return pl.ds(pl.multiple_of(plane(d) * tl + cc * half, half), half)

    def r0_rows(d):
        return pl.ds(d * half, half)

    for d in order + [0]:
        slope_block(d)

    for d in order + [0]:
        at = d_block(plane(d))
        ug[at, :] = jnp.transpose(jnp.dot(s_t[...], tx[:, at], preferred_element_type=F32)).astype(BF16)
        if d:
            send(ug.at[at, :], ru_ref.at[:, up_cols(z)], dev(zz=plane(d)), ("ru", R - d))
        else:
            ru_ref[:, up_cols(z)] = ug[at, :]

    for d in order + [0]:
        @pl.loop(0, tl // step)
        def _(i):
            at = pl.ds(pl.multiple_of(plane(d) * tl + i * step, step), step)
            part[at, :] = contract_last(slopes[at, :], wu[...]).astype(BF16)
        send(part.at[half_rows(d, 1 - c), :], r0.at[r0_rows(d), :], dev(cc=1 - c), ("r0", d))

    def added(*terms):
        total = terms[0].astype(F32)
        for term in terms[1:]:
            total = total + term.astype(F32)
        return total.astype(BF16)

    def core_sum(d):
        arrived(r0.at[r0_rows(d), :], ("r0", d))
        for ff in (f1, f3, f, f2):
            at = rows(plane(d), ff, c)
            part[at, :] = added(part[at, :], r0[pl.ds(pl.multiple_of(d * half + ff * pr, pr), pr), :])
        for k, ff in ((0, f1), (1, f3)):
            send(part.at[rows(plane(d), ff, c), :], r1.at[d, k], dev(ff=f1), ("r1", d, k))

    def first_sum(d):
        for k, ff in ((1, f2), (0, f)):
            at = rows(plane(d), ff, c)
            arrived(r1.at[d, k], ("r1", d, k))
            part[at, :] = added(part[at, :], r1[d, k])
            if k:
                send(part.at[at, :], r2.at[d], dev(ff=f2), ("r2", d))

    def second_sum(d):
        at = rows(plane(d), f, c)
        arrived(r2.at[d], ("r2", d))
        part[at, :] = added(part[at, :], r2[d])
        if d:
            send(part.at[at, :], r3.at[R - d], dev(zz=plane(d)), ("r3", R - d))

    turns = order + [0]
    chain = (core_sum, first_sum, second_sum)
    for i in range(len(turns) + 2):
        for back in (2, 1, 0):
            if 0 <= i - back < len(turns):
                chain[back](turns[i - back])

    for d in order:
        arrived(r3.at[d], ("r3", d))
    ig_ref[pl.ds(pl.multiple_of((c * 4 + f) * pr, pr), pr), :] = added(
        part[rows(z, f, c), :], *[r3[d] for d in order])
    for stage in spread(ig_ref, ("ig",), None):
        stage()

    for d in order:
        arrived(rd_ref.at[up_cols(plane(d)), :], ("rd", d))
        arrived(ru_ref.at[:, up_cols(plane(d))], ("ru", d))
    for copy in pending:
        copy.wait_send()
    assert len(pending) <= SEMS and len(keys) <= SEMS


def in_planes(R, hidden_in, cotangent, w_up, w_down):
    tl, D = hidden_in.shape
    dl, fl = w_up.shape
    T, h, pr = tl * R, fl // R, tl // 8
    vmem = pl.BlockSpec(memory_space=pltpu.VMEM)
    input_grad, up, down = pl.pallas_call(
        functools.partial(kernel, R),
        out_shape=(
            jax.ShapeDtypeStruct((tl, D), BF16),
            jax.ShapeDtypeStruct((dl, fl), BF16),
            jax.ShapeDtypeStruct((fl, dl), BF16),
        ),
        in_specs=[pl.BlockSpec(memory_space=pl.ANY)] * 4,
        out_specs=(vmem, vmem, vmem),
        scratch_shapes=[
            pltpu.VMEM((T, D), BF16),
            pltpu.VMEM((T, D), BF16),
            pltpu.VMEM((D, h), BF16),
            pltpu.VMEM((h, D), BF16),
            pltpu.VMEM((T, h), F32),
            pltpu.VMEM((T, h), BF16),
            pltpu.VMEM((h, T), BF16),
            pltpu.VMEM((h, T), BF16),
            pltpu.VMEM((T, D), BF16),
            pltpu.VMEM((R * 4 * pr, D), BF16),
            pltpu.VMEM((R, 2, pr, D), BF16),
            pltpu.VMEM((R, pr, D), BF16),
            pltpu.VMEM((R, pr, D), BF16),
            pltpu.VMEM((D, h), BF16),
            pltpu.VMEM((h, D), BF16),
            pltpu.SemaphoreType.DMA((SEMS,)),
            pltpu.SemaphoreType.DMA((SEMS,)),
            pltpu.SemaphoreType.DMA((4,)),
        ],
        compiler_params=pltpu.CompilerParams(
            collective_id=0, has_side_effects=True, vmem_limit_bytes=65000 * 1024
        ),
    )(hidden_in, cotangent, w_up, w_down)
    return input_grad, up.astype(F32), down.astype(F32)


def solution(mesh):
    R, F, C = (mesh.shape[name] for name in ("rep", "fs", "tp"))
    body = functools.partial(in_planes, R) if (F, C) == (4, 2) else plain
    return jax.shard_map(
        body,
        mesh=mesh,
        in_specs=(P("rep", None), P("rep", None), P("rep", ("fs", "tp")), P(("fs", "tp"), "rep")),
        out_specs=(P("rep", None), P("rep", ("fs", "tp")), P(("fs", "tp"), "rep")),
        check_vma=False,
    )
```

time: 415 us -> 201 us (0.48)
  waiting for transfers between devices: 360 us -> 0 us
  Pallas kernels: 0 us -> 194 us
  matrix products: 29.3 us -> 0 us
  between operations: 13.8 us -> 0.65 us
    pallas_call x0 -> x1, Pallas kernels: none -> 194 us  [in_planes(): pl.pallas_call(functools.partial(kernel, R), out_shape=(jax.ShapeDtypeStr...]
    all_gather x2 -> x0, waiting for transfers between devices: 155 us -> none  [the longest x1 80 us: on_device(): up_full = lax.all_gather(w_up, 'rep', axis=0, tiled=True)]
    reduce_scatter x2 -> x0, waiting for transfers between devices: 141 us -> none  [the longest x1 76.9 us: on_device(): lax.psum_scatter(contract_first(cotangent, hidden).astype(jnp.bfloat16),...]
    psum x1 -> x0, waiting for transfers between devices: 62.6 us -> none  [on_device(): lax.psum(partial_sum, ('fs', 'tp')).astype(jnp.float32).astype(jnp.bfloat16)]
    dot_general x5 -> x0, matrix products: 29.3 us -> none  [the longest x2 12.5 us: contract_last(): lax.dot_general(left, right, (((1,), (1,)), ((), ())), preferred_element_...]
    convert_element_type x0 -> x2, other arithmetic: none -> 4.49 us  [in_planes(): return (input_grad, up.astype(F32), down.astype(F32))]
  transfers between devices with their start and end apart: 5 -> 0, of which waited for: 5 -> 0; matrix products, arithmetic and copies ran while one was open for 6% -> 0% of each run, Pallas kernels for 0% -> 0%
where the time goes in v1:
time: 201 us
  Pallas kernels  194 us (97%)
  other arithmetic  4.49 us (2%)
  local copies, waits for them, and re-layouts  2.06 us (1%)
    pallas_call x1, Pallas kernels, in_planes(): pl.pallas_call(functools.partial(kernel, R), out_shape=(jax.ShapeDtypeStr...  194 us
    convert_element_type x2, other arithmetic, in_planes(): return (input_grad, up.astype(F32), down.astype(F32))  4.49 us

profile of v1, /device:TPU:25, one launch (start us, length us, event | category | flops | bytes accessed | tf_op | source)
XLA Modules:
  0.0 201.0 jit_solution(15047799281196840410)
XLA Ops:
  0.6 193.8 %shard_map.67 = (bf16[512,2048]{1,0:T(8,128)(2,1)}, bf16[512,1024]{1,0:T(8,128)(2,1)}, bf16[1024,512]{1,0:T(8,128)(2,1)}) custom-call(bf16[512,2048]{1,0:T(8,128)(2,1)} %x_ref.1, bf16[512,2048]{1,0:T(8,128)(2,1)} %g_ref.1, bf16[512,1024]{1,0:T(8,128)(2,1)} %wu_in.1, bf16[1024,512]{1,0:T(8,128)(2,1)} %wd_in.1), custom_call_target="tpu_custom_call" | custom-call | tf_op jit(solution)/shard_map/pallas_call | solution.py:294
  194.4 0.0 copy-start.1
  194.4 2.9 %convert_element_type.6 = f32[512,1024]{1,0:T(8,128)} convert(bf16[512,1024]{1,0:T(8,128)(2,1)} %get-tuple-element.7) | non-fusion elementwise | flops 524288 | bytes 3145728 | tf_op jit(solution)/shard_map/convert_element_type | solution.py:327
  197.3 0.0 copy-done.1
  197.3 0.0 copy-start
  197.3 1.6 convert_element_type.7
  198.9 0.7 copy-done
  199.6 1.3 copy.8
Async XLA Ops:
  194.4 2.9 %copy-start.1 = (bf16[1024,512]{1,0:T(8,128)(2,1)S(1)}, bf16[1024,512]{1,0:T(8,128)(2,1)}, u32[]{:S(2)}) copy-start(bf16[1024,512]{1,0:T(8,128)(2,1)} %get-tuple-element.8) | copy-start | bytes 3145732
  197.3 2.3 %copy-start = (bf16[512,2048]{1,0:T(8,128)(2,1)S(1)}, bf16[512,2048]{1,0:T(8,128)(2,1)}, u32[]{:S(2)}) copy-start(bf16[512,2048]{1,0:T(8,128)(2,1)} %get-tuple-element.12) | copy-start | bytes 6291460

commit v2 on v1

v2 whole, which is shorter than its diff:
```python
import functools

import jax
import jax.numpy as jnp
from jax import lax
from jax.experimental import pallas as pl
from jax.experimental.pallas import tpu as pltpu
from jax.sharding import PartitionSpec as P

MESH = pl.DeviceIdType.MESH
BF16, F32 = jnp.bfloat16, jnp.float32


def contract_last(left, right):
    return lax.dot_general(left, right, (((1,), (1,)), ((), ())), preferred_element_type=F32)


def contract_first(left, right):
    return lax.dot_general(left, right, (((0,), (0,)), ((), ())), preferred_element_type=F32)


def plain(hidden_in, cotangent, w_up, w_down):
    up_full = lax.all_gather(w_up, "rep", axis=0, tiled=True)
    back_grad = contract_last(cotangent, lax.all_gather(w_down, "rep", axis=1, tiled=True))
    preact = jnp.dot(hidden_in, up_full, preferred_element_type=F32)
    active = jnp.maximum(preact, 0.0)
    hidden = (active * active).astype(BF16)
    slopes = (2.0 * active * back_grad).astype(BF16)
    grad_upper = lax.psum_scatter(
        contract_first(hidden_in, slopes).astype(BF16), "rep", scatter_dimension=0, tiled=True
    ).astype(F32)
    lower_rows = lax.psum_scatter(
        contract_first(cotangent, hidden).astype(BF16), "rep", scatter_dimension=0, tiled=True
    ).astype(F32)
    partial_sum = contract_last(slopes, up_full).astype(BF16)
    input_grad = lax.psum(partial_sum, ("fs", "tp")).astype(F32).astype(BF16)
    return (input_grad, grad_upper, lower_rows.T)


SEMS = 256


def kernel(
    R, x_ref, g_ref, wu_in, wd_in,
    ig_ref, ru_ref, rd_ref,
    tx, tg, wu, wd, act, slopes, s_t, h_t, part, r0, r1, r2, r3, ug, dg,
    send_sems, recv_sems, local_sems,
):
    z, f, c = lax.axis_index("rep"), lax.axis_index("fs"), lax.axis_index("tp")
    tl, D = x_ref.shape
    dl, fl = wu_in.shape
    h = fl // R
    pr = tl // 8
    xx, yy = lax.rem(f, 2), lax.div(f, 2)
    fx, fy = yy * 2 + (1 - xx), (1 - yy) * 2 + xx
    f1 = fx * (1 - c) + fy * c
    f2 = fy * (1 - c) + fx * c
    f3 = 3 - f

    edge = jnp.minimum(z, R - 1 - z)
    far = jnp.where(z < R - 1 - z, 1, -1)

    def plane_at(slot):
        both = z + (slot // 2 + 1) * (2 * (slot % 2) - 1) * far
        return jnp.where(slot < 2 * edge, both, z + far * (slot + 1 - edge))

    near_first = [plane_at(slot) for slot in range(R - 1)]
    far_first = near_first[::-1]

    def beyond(p):
        return jnp.logical_or(jnp.logical_and(p < z, z < R - 1), jnp.logical_and(p > z, z > 0))

    def past(p):
        return jnp.where(p < z, z + 1, z - 1)

    def toward(p):
        return jnp.where(p > z, z + 1, z - 1)

    pending = []
    keys = {}

    def key_of(key, p):
        return keys.setdefault(key, len(keys)) * R + p

    def dev(zz=None, ff=None, cc=None):
        return {"rep": z if zz is None else zz, "fs": f if ff is None else ff, "tp": c if cc is None else cc}

    def send(src, dst, device, key, p, when=None):
        copy = pltpu.make_async_remote_copy(
            src_ref=src, dst_ref=dst, send_sem=send_sems.at[len(pending)],
            recv_sem=recv_sems.at[key_of(key, p)], device_id=device, device_id_type=MESH)
        pending.append((copy, when))
        if when is None:
            copy.start()
        else:
            pl.when(when)(copy.start)

    def arrived(dst, key, p):
        pltpu.make_async_remote_copy(
            src_ref=dst, dst_ref=dst, send_sem=send_sems.at[0],
            recv_sem=recv_sems.at[key_of(key, p)], device_id=dev(cc=1 - c), device_id_type=MESH).wait_recv()

    def rows(zz, ff, cc):
        return pl.ds(pl.multiple_of(zz * tl + (cc * 4 + ff) * pr, pr), pr)

    def piece_rows(ff, cc):
        return pl.ds(pl.multiple_of((cc * 4 + ff) * pr, pr), pr)

    barrier = pltpu.get_barrier_semaphore()
    near = [dev(zz=lax.rem(z + d, R)) for d in range(1, R)] + [dev(ff=fx), dev(ff=fy), dev(cc=1 - c)]
    for device in near:
        pl.semaphore_signal(barrier, inc=1, device_id=device, device_id_type=MESH)
    pl.semaphore_wait(barrier, len(near))

    tokens = (tx, tg)
    sources = (x_ref, g_ref)

    def up_cols(zz):
        return pl.ds(pl.multiple_of(zz * h, h), h)

    def d_block(zz):
        return pl.ds(pl.multiple_of(zz * dl, dl), dl)

    for a in (0, 1):
        for to, there in ((z + 1, z < R - 1), (z - 1, z > 0)):
            send(sources[a].at[piece_rows(f, c), :], tokens[a].at[rows(z, f, c), :],
                 dev(zz=to), ("tok", a, 0), z, when=there)

    own_rows = pl.ds(pl.multiple_of(z * tl, tl), tl)
    local = [
        pltpu.make_async_copy(x_ref, tx.at[own_rows, :], local_sems.at[0]),
        pltpu.make_async_copy(g_ref, tg.at[own_rows, :], local_sems.at[1]),
        pltpu.make_async_copy(wu_in.at[:, up_cols(z)], wu.at[d_block(z), :], local_sems.at[2]),
        pltpu.make_async_copy(wd_in.at[up_cols(z), :], wd.at[:, d_block(z)], local_sems.at[3]),
    ]
    for copy in local:
        copy.start()

    def send_weights(planes):
        for p in planes:
            send(wu_in.at[:, up_cols(p)], wu.at[d_block(z), :], dev(zz=p), ("wu",), z)
        for p in planes:
            send(wd_in.at[up_cols(p), :], wd.at[:, d_block(z)], dev(zz=p), ("wd",), z)

    def spread(at, tag, p):
        def first():
            mine = at(f, c)
            send(mine, mine, dev(ff=f1), tag + (1,), p)
            send(mine, mine, dev(ff=f2), tag + (2,), p)
            send(mine, mine, dev(cc=1 - c), tag + (4,), p)

        def second():
            p1, p2 = at(f1, c), at(f2, c)
            arrived(p1, tag + (1,), p)
            send(p1, p1, dev(ff=f2), tag + (3,), p)
            send(p1, p1, dev(cc=1 - c), tag + (5,), p)
            arrived(p2, tag + (2,), p)
            send(p2, p2, dev(cc=1 - c), tag + (6,), p)

        def third():
            p3 = at(f3, c)
            arrived(p3, tag + (3,), p)
            send(p3, p3, dev(cc=1 - c), tag + (7,), p)

        def last():
            for k, ff in ((4, f), (5, f2), (6, f1), (7, f3)):
                arrived(at(ff, 1 - c), tag + (k,), p)

        return first, second, third, last

    lasts = {}
    stages = []
    for a in (0, 1):
        for slot, p in enumerate(near_first):
            first, second, third, last = spread(
                lambda ff, cc, a=a, p=p: tokens[a].at[rows(p, ff, cc), :], ("tok", a), p)

            def opening(a=a, p=p, first=first):
                mine = tokens[a].at[rows(p, f, c), :]
                arrived(mine, ("tok", a, 0), p)
                send(mine, mine, dev(zz=past(p)), ("tok", a, 0), p, when=beyond(p))
                first()

            stages.append((opening, second, third))
            lasts[a, slot] = last
    step = min(tl, 256)

    def up_block(p):
        @pl.loop(0, tl // step)
        def _(i):
            at = pl.ds(pl.multiple_of(p * tl + i * step, step), step)
            active = jnp.maximum(jnp.dot(tx[at, :], wu[...], preferred_element_type=F32), 0.0)
            act[at, :] = active
            h_t[:, at] = jnp.transpose(active * active).astype(BF16)

    def up_blocks():
        for copy in local:
            copy.wait()
        for p in near_first:
            arrived(wu.at[d_block(p), :], ("wu",), p)
        up_block(z)
        for slot, p in enumerate(near_first):
            lasts[0, slot]()
            up_block(p)

    for i in range(len(stages) + 2):
        if i == len(stages) + 1:
            up_blocks()
        for back in (0, 1, 2):
            if 0 <= i - back < len(stages):
                stages[i - back][back]()
        if i == R - 1:
            send_weights(far_first[:R // 2])
        if i == len(stages) - 1:
            send_weights(far_first[R // 2:])

    for slot in range(R - 1):
        lasts[1, slot]()

    def down_part(p):
        at = d_block(p)
        dg[:, at] = jnp.dot(h_t[...], tg[:, at], preferred_element_type=F32).astype(BF16)

    for p in far_first:
        down_part(p)
        send(dg.at[:, d_block(p)], rd_ref.at[up_cols(z), :], dev(zz=p), ("rd",), z)
    down_part(z)
    rd_ref[up_cols(z), :] = dg[:, d_block(z)]

    for p in near_first:
        arrived(wd.at[:, d_block(p)], ("wd",), p)

    half = 4 * pr
    blocks = far_first + [z]

    def r0_rows(j, ff=None):
        if ff is None:
            return pl.ds(j * half, half)
        return pl.ds(pl.multiple_of(j * half + ff * pr, pr), pr)

    def added(*terms):
        total = terms[0].astype(F32)
        for term in terms[1:]:
            total = total + term.astype(F32)
        return total.astype(BF16)

    def core_sum(j):
        p = blocks[j]
        arrived(r0.at[r0_rows(j), :], ("r0", j), 0)
        for k, ff in ((1, f3), (0, f1), (None, f2), (None, f)):
            at = rows(p, ff, c)
            part[at, :] = added(part[at, :], r0[r0_rows(j, ff), :])
            if k is not None:
                send(part.at[at, :], r1.at[j, k], dev(ff=f1), ("r1", j, k), 0)

    for j, p in enumerate(blocks):
        @pl.loop(0, tl // step)
        def _(i, p=p):
            at = pl.ds(pl.multiple_of(p * tl + i * step, step), step)
            value = 2.0 * act[at, :] * contract_last(tg[at, :], wd[...])
            slopes[at, :] = value.astype(BF16)
            s_t[:, at] = jnp.transpose(value).astype(BF16)
            part[at, :] = contract_last(slopes[at, :], wu[...]).astype(BF16)

        theirs = pl.ds(pl.multiple_of(p * tl + (1 - c) * half, half), half)
        send(part.at[theirs, :], r0.at[r0_rows(j), :], dev(cc=1 - c), ("r0", j), 0)
        if j:
            core_sum(j - 1)
    core_sum(R - 1)

    def first_sum(j):
        for k, ff in ((1, f2), (0, f)):
            at = rows(blocks[j], ff, c)
            arrived(r1.at[j, k], ("r1", j, k), 0)
            part[at, :] = added(part[at, :], r1[j, k])
            if k:
                send(part.at[at, :], r2.at[j], dev(ff=f2), ("r2", j), 0)

    def second_sum(j):
        p = blocks[j]
        at = rows(p, f, c)
        arrived(r2.at[j], ("r2", j), 0)
        part[at, :] = added(part[at, :], r2[j])

    def line_sum(j):
        p = blocks[j]
        at = rows(p, f, c)
        side = jnp.where(p > z, 0, 1)

        @pl.when(beyond(p))
        def _():
            arrived(r3.at[p, side], ("r3",), p * 2 + side)
            part[at, :] = added(part[at, :], r3[p, side])

        send(part.at[at, :], r3.at[p, side], dev(zz=toward(p)), ("r3",), p * 2 + side)

    def own_sum():
        at = rows(z, f, c)
        for side, there in ((0, z > 0), (1, z < R - 1)):
            @pl.when(there)
            def _(side=side):
                arrived(r3.at[z, side], ("r3",), z * 2 + side)
                part[at, :] = added(part[at, :], r3[z, side])
        ig_ref[piece_rows(f, c), :] = part[at, :]

    def up_part(p):
        at = d_block(p)
        ug[at, :] = jnp.transpose(jnp.dot(s_t[...], tx[:, at], preferred_element_type=F32)).astype(BF16)

    chain = (first_sum, second_sum, line_sum)
    key_of(("r3",), 0)
    key_of("above", 0)
    for i in range(R + 2):
        for back in (2, 1, 0):
            j = i - back
            if 0 <= j < R and not (back == 2 and j == R - 1):
                chain[back](j)
        if i < R - 1:
            p = far_first[i]
            up_part(p)
            send(ug.at[d_block(p), :], ru_ref.at[:, up_cols(z)], dev(zz=p), ("ru",), z)
        if i == R - 1:
            up_part(z)
            ru_ref[:, up_cols(z)] = ug[d_block(z), :]

    own_sum()
    for stage in spread(lambda ff, cc: ig_ref.at[piece_rows(ff, cc), :], ("ig",), 0):
        stage()

    for p in near_first:
        arrived(rd_ref.at[up_cols(p), :], ("rd",), p)
        arrived(ru_ref.at[:, up_cols(p)], ("ru",), p)
    for copy, when in pending:
        if when is None:
            copy.wait_send()
        else:
            pl.when(when)(copy.wait_send)
    assert len(pending) <= SEMS and len(keys) * R <= SEMS


def in_planes(R, hidden_in, cotangent, w_up, w_down):
    tl, D = hidden_in.shape
    dl, fl = w_up.shape
    T, h, pr = tl * R, fl // R, tl // 8
    vmem = pl.BlockSpec(memory_space=pltpu.VMEM)
    input_grad, up, down = pl.pallas_call(
        functools.partial(kernel, R),
        out_shape=(
            jax.ShapeDtypeStruct((tl, D), BF16),
            jax.ShapeDtypeStruct((dl, fl), BF16),
            jax.ShapeDtypeStruct((fl, dl), BF16),
        ),
        in_specs=[pl.BlockSpec(memory_space=pl.ANY)] * 4,
        out_specs=(vmem, vmem, vmem),
        scratch_shapes=[
            pltpu.VMEM((T, D), BF16),
            pltpu.VMEM((T, D), BF16),
            pltpu.VMEM((D, h), BF16),
            pltpu.VMEM((h, D), BF16),
            pltpu.VMEM((T, h), F32),
            pltpu.VMEM((T, h), BF16),
            pltpu.VMEM((h, T), BF16),
            pltpu.VMEM((h, T), BF16),
            pltpu.VMEM((T, D), BF16),
            pltpu.VMEM((R * 4 * pr, D), BF16),
            pltpu.VMEM((R, 2, pr, D), BF16),
            pltpu.VMEM((R, pr, D), BF16),
            pltpu.VMEM((R, 2, pr, D), BF16),
            pltpu.VMEM((D, h), BF16),
            pltpu.VMEM((h, D), BF16),
            pltpu.SemaphoreType.DMA((SEMS,)),
            pltpu.SemaphoreType.DMA((SEMS,)),
            pltpu.SemaphoreType.DMA((4,)),
        ],
        compiler_params=pltpu.CompilerParams(
            collective_id=0, has_side_effects=True, vmem_limit_bytes=65000 * 1024
        ),
    )(hidden_in, cotangent, w_up, w_down)
    return input_grad, up.astype(F32), down.astype(F32)


def solution(mesh):
    R, F, C = (mesh.shape[name] for name in ("rep", "fs", "tp"))
    body = functools.partial(in_planes, R) if (F, C) == (4, 2) else plain
    return jax.shard_map(
        body,
        mesh=mesh,
        in_specs=(P("rep", None), P("rep", None), P("rep", ("fs", "tp")), P(("fs", "tp"), "rep")),
        out_specs=(P("rep", None), P("rep", ("fs", "tp")), P(("fs", "tp"), "rep")),
        check_vma=False,
    )
```

time: 201 us -> 173 us (0.86); the launches traced: 201 us -> 170 us
  Pallas kernels: 194 us -> 163 us
    pallas_call x1, Pallas kernels: 194 us -> 163 us  [in_planes(): pl.pallas_call(functools.partial(kernel, R), out_shape=(jax.ShapeDtypeStr...]
where the time goes in v2:
time: 173 us; the launch traced here: 170 us
  Pallas kernels  163 us (94%)
  other arithmetic  4.49 us (3%)
  local copies, waits for them, and re-layouts  2.06 us (1%)
    pallas_call x1, Pallas kernels, in_planes(): pl.pallas_call(functools.partial(kernel, R), out_shape=(jax.ShapeDtypeStr...  163 us
    convert_element_type x2, other arithmetic, in_planes(): return (input_grad, up.astype(F32), down.astype(F32))  4.49 us

profile of v2, /device:TPU:25, one launch (start us, length us, event | category | flops | bytes accessed | tf_op | source)
XLA Modules:
  0.0 169.9 jit_solution(8849014222086324775)
XLA Ops:
  0.6 162.7 %shard_map.67 = (bf16[512,2048]{1,0:T(8,128)(2,1)}, bf16[512,1024]{1,0:T(8,128)(2,1)}, bf16[1024,512]{1,0:T(8,128)(2,1)}) custom-call(bf16[512,2048]{1,0:T(8,128)(2,1)} %x_ref.1, bf16[512,2048]{1,0:T(8,128)(2,1)} %g_ref.1, bf16[512,1024]{1,0:T(8,128)(2,1)} %wu_in.1, bf16[1024,512]{1,0:T(8,128)(2,1)} %wd_in.1), custom_call_target="tpu_custom_call" | custom-call | tf_op jit(solution)/shard_map/pallas_call | solution.py:346
  163.4 0.0 copy-start.1
  163.4 2.9 %convert_element_type.6 = f32[512,1024]{1,0:T(8,128)} convert(bf16[512,1024]{1,0:T(8,128)(2,1)} %get-tuple-element.7) | non-fusion elementwise | flops 524288 | bytes 3145728 | tf_op jit(solution)/shard_map/convert_element_type | solution.py:379
  166.3 0.0 copy-done.1
  166.3 0.0 copy-start
  166.3 1.6 convert_element_type.7
  167.9 0.7 copy-done
  168.6 1.3 copy.8
Async XLA Ops:
  163.4 2.9 %copy-start.1 = (bf16[1024,512]{1,0:T(8,128)(2,1)S(1)}, bf16[1024,512]{1,0:T(8,128)(2,1)}, u32[]{:S(2)}) copy-start(bf16[1024,512]{1,0:T(8,128)(2,1)} %get-tuple-element.8) | copy-start | bytes 3145732
  166.3 2.3 %copy-start = (bf16[512,2048]{1,0:T(8,128)(2,1)S(1)}, bf16[512,2048]{1,0:T(8,128)(2,1)}, u32[]{:S(2)}) copy-start(bf16[512,2048]{1,0:T(8,128)(2,1)} %get-tuple-element.12) | copy-start | bytes 6291460

commit v3 on v2

--- a/solution.py
+++ b/solution.py
@@ -324,8 +324,13 @@
             ru_ref[:, up_cols(z)] = ug[d_block(z), :]
 
     own_sum()
-    for stage in spread(lambda ff, cc: ig_ref.at[piece_rows(ff, cc), :], ("ig",), 0):
-        stage()
+    def part_of(n):
+        rows_of = lambda ff, cc: pl.ds(pl.multiple_of((cc * 4 + ff) * pr + n * (pr // 2), pr // 2), pr // 2)
+        return spread(lambda ff, cc: ig_ref.at[rows_of(ff, cc), :], ("ig", n), 0)
+
+    for pair in zip(part_of(0), part_of(1)):
+        for stage in pair:
+            stage()
 
     for p in near_first:
         arrived(rd_ref.at[up_cols(p), :], ("rd",), p)

time: 173 us -> 171 us (0.988)
  Pallas kernels: 163 us -> 161 us
where the time goes in v3:
time: 171 us; the launch traced here: 168 us
  Pallas kernels  161 us (94%)
  other arithmetic  4.49 us (3%)
  local copies, waits for them, and re-layouts  2.06 us (1%)
    pallas_call x1, Pallas kernels, in_planes(): pl.pallas_call(functools.partial(kernel, R), out_shape=(jax.ShapeDtypeStr...  161 us
    convert_element_type x2, other arithmetic, in_planes(): return (input_grad, up.astype(F32), down.astype(F32))  4.49 us

profile of v3, /device:TPU:25, one launch (start us, length us, event | category | flops | bytes accessed | tf_op | source)
XLA Modules:
  0.0 168.4 jit_solution(10026405444148155733)
XLA Ops:
  0.6 161.2 %shard_map.67 = (bf16[512,2048]{1,0:T(8,128)(2,1)}, bf16[512,1024]{1,0:T(8,128)(2,1)}, bf16[1024,512]{1,0:T(8,128)(2,1)}) custom-call(bf16[512,2048]{1,0:T(8,128)(2,1)} %x_ref.1, bf16[512,2048]{1,0:T(8,128)(2,1)} %g_ref.1, bf16[512,1024]{1,0:T(8,128)(2,1)} %wu_in.1, bf16[1024,512]{1,0:T(8,128)(2,1)} %wd_in.1), custom_call_target="tpu_custom_call" | custom-call | tf_op jit(solution)/shard_map/pallas_call | solution.py:351
  161.8 0.0 copy-start.1
  161.8 2.9 %convert_element_type.6 = f32[512,1024]{1,0:T(8,128)} convert(bf16[512,1024]{1,0:T(8,128)(2,1)} %get-tuple-element.7) | non-fusion elementwise | flops 524288 | bytes 3145728 | tf_op jit(solution)/shard_map/convert_element_type | solution.py:384
  164.7 0.0 copy-done.1
  164.7 0.0 copy-start
  164.7 1.6 convert_element_type.7
  166.3 0.7 copy-done
  167.0 1.3 copy.8
Async XLA Ops:
  161.8 2.9 %copy-start.1 = (bf16[1024,512]{1,0:T(8,128)(2,1)S(1)}, bf16[1024,512]{1,0:T(8,128)(2,1)}, u32[]{:S(2)}) copy-start(bf16[1024,512]{1,0:T(8,128)(2,1)} %get-tuple-element.8) | copy-start | bytes 3145732
  164.7 2.3 %copy-start = (bf16[512,2048]{1,0:T(8,128)(2,1)S(1)}, bf16[512,2048]{1,0:T(8,128)(2,1)}, u32[]{:S(2)}) copy-start(bf16[512,2048]{1,0:T(8,128)(2,1)} %get-tuple-element.12) | copy-start | bytes 6291460
